TPU v7x, 32 devices: a whole 2x2x4 slice. The times are simulated.
32 devices in a mesh: sp: 8 (over z, y), tp: 4 (over x, core).
Axes of the slice: x: 2, y: 2, z: 4, core: 2. Of those that a mesh axis runs over, the one named last changes fastest.
Arguments:
- tokens: bfloat16 [2048, 4096], P(('sp', 'tp')), may hold values from -6 to 6, as said below
- query_one: bfloat16 [4096, 1024], P('sp', 'tp'), may hold values from -0.125 to 0.125
- query_two: bfloat16 [4096, 1024], P('sp', 'tp'), may hold values from -0.125 to 0.125
- key_one: bfloat16 [4096, 1024], P('sp', 'tp'), may hold values from -0.125 to 0.125
- key_two: bfloat16 [4096, 1024], P('sp', 'tp'), may hold values from -0.125 to 0.125
- value_weight: bfloat16 [4096, 2048], P('sp', 'tp'), may hold values from -0.09375 to 0.09375
- out_weight: bfloat16 [2048, 4096], P('tp', 'sp'), may hold values from -0.125 to 0.125
- lambdas: float32 [8], P('tp'), may hold values from 0.3 to 0.8
- head_gain: float32 [256], replicated, may hold values from 0.1 to 1.9
Outputs:
- layer_out: bfloat16 [2048, 4096], P(('sp', 'tp'))
Inputs may be any that keep to these rules, and one draw needn't show every extreme that they name: `tokens`: the features' mean changes between 16 equal spans of the sequence.
All inputs are finite; a program needn't handle non-finite values.
Results may differ from a plain program's by a relative error of at most 0.013.
The roundings to bfloat16 on the way count: a program that leaves them out, or rounds other values in their place, can miss the bound.
Values may be sent and summed in bfloat16 or wider, within the bound.
No kernel may reach another device: no remote copies, remote signals or barrier semaphores. Data moves between devices by JAX's collectives and lax.ppermute only.
A program may use at most 128 MiB of HBM per device.

v0:
```python
import jax
import jax.numpy as jnp
from jax import lax
from jax.sharding import PartitionSpec as P

QK = 128
V = 256
ROPE_BASE = 500000.0
EPS_NORM = 0.02


def rotate(values, positions):
    half_dim = values.shape[-1] // 2
    inverse = 1.0 / ROPE_BASE ** (
        jnp.arange(0, 2 * half_dim, 2, dtype=jnp.float32) / (2 * half_dim)
    )
    angles = positions.astype(jnp.float32)[:, None] * inverse[None, :]
    cos_part = jnp.cos(angles)[:, None, :]
    sin_part = jnp.sin(angles)[:, None, :]
    first_half = values[..., :half_dim]
    second_half = values[..., half_dim:]
    return jnp.concatenate(
        [
            first_half * cos_part - second_half * sin_part,
            second_half * cos_part + first_half * sin_part,
        ],
        axis=-1,
    )


def unchanged(carried):
    return carried


def on_device(
    tokens, query_one, query_two, key_one, key_two, value_weight, out_weight, lambdas, head_gain
):
    tp_count = lax.axis_size("tp")
    sp_index = lax.axis_index("sp")
    own_rows = tokens.shape[0]
    local_len = own_rows * tp_count
    half_len = local_len // 2
    heads_here = lambdas.shape[0]
    gathered = lax.all_gather(tokens, "tp", axis=0, tiled=True)
    row_ids = jnp.arange(local_len, dtype=jnp.int32)
    query_pos = sp_index * local_len + row_ids
    pieces = (
        lax.all_gather(query_one, "sp", axis=0, tiled=True),
        lax.all_gather(query_two, "sp", axis=0, tiled=True),
        lax.all_gather(key_one, "sp", axis=0, tiled=True),
        lax.all_gather(key_two, "sp", axis=0, tiled=True),
        lax.all_gather(value_weight, "sp", axis=0, tiled=True),
    )
    projected = tuple(
        (
            jnp.dot(gathered, weight_piece, preferred_element_type=jnp.float32)
            for weight_piece in pieces
        )
    )

    def turned(product):
        return rotate(product.reshape(local_len, heads_here, QK), query_pos).astype(jnp.bfloat16)

    q_one = turned(projected[0])
    q_two = turned(projected[1])
    k_one = turned(projected[2]).reshape(local_len, heads_here * QK)
    k_two = turned(projected[3]).reshape(local_len, heads_here * QK)
    values = projected[4].astype(jnp.bfloat16)
    scale = QK ** (-0.5)
    pieces = (
        lax.all_gather(k_one, "sp", axis=0, tiled=True),
        lax.all_gather(k_two, "sp", axis=0, tiled=True),
        lax.all_gather(values, "sp", axis=0, tiled=True),
    )
    key_count = pieces[0].shape[0]
    global_ids = jnp.arange(key_count, dtype=jnp.int32)
    shard_ids = global_ids // local_len
    within = global_ids % local_len
    key_pos = shard_ids * local_len + within
    key_sets = (
        pieces[0].reshape(key_count, heads_here, QK),
        pieces[1].reshape(key_count, heads_here, QK),
    )
    value_rows = pieces[2].reshape(key_count, heads_here, V)
    row_tops = jnp.full((2, heads_here, local_len), -1e30, jnp.float32)
    totals = jnp.zeros((2, heads_here, local_len), jnp.float32)
    accums = jnp.zeros((2, heads_here, local_len, V), jnp.float32)
    new_parts = []
    for segment in range(2):
        low_row = segment * half_len
        seg_pos = query_pos[low_row : low_row + half_len]
        queries = (q_one[low_row : low_row + half_len], q_two[low_row : low_row + half_len])
        carried = (
            row_tops[:, :, low_row : low_row + half_len],
            totals[:, :, low_row : low_row + half_len],
            accums[:, :, low_row : low_row + half_len],
        )

        def update(carried, queries=queries, seg_pos=seg_pos):
            allowed = key_pos[None, :] <= seg_pos[:, None]
            out_tops, out_totals, out_accums = ([], [], [])
            for map_index in range(2):
                scores = (
                    jnp.einsum(
                        "qhd,khd->hqk",
                        queries[map_index],
                        key_sets[map_index],
                        preferred_element_type=jnp.float32,
                    )
                    * scale
                )
                masked = jnp.where(allowed[None], scores, -1e30)
                old_top = carried[0][map_index]
                new_top = jnp.maximum(old_top, jnp.max(masked, axis=-1))
                exp_weights = jnp.where(allowed[None], jnp.exp(scores - new_top[..., None]), 0.0)
                new_total = jnp.sum(exp_weights, axis=-1)
                new_accum = jnp.einsum(
                    "hqk,khv->hqv",
                    exp_weights.astype(jnp.bfloat16),
                    value_rows,
                    preferred_element_type=jnp.float32,
                )
                out_tops.append(new_top)
                out_totals.append(new_total)
                out_accums.append(new_accum)
            return (jnp.stack(out_tops), jnp.stack(out_totals), jnp.stack(out_accums))

        needed = jnp.min(key_pos) <= jnp.max(seg_pos)
        new_parts.append(lax.cond(needed, update, unchanged, carried))
    row_tops, totals, accums = tuple(
        (
            jnp.concatenate([new_part[member] for new_part in new_parts], axis=2)
            for member in range(3)
        )
    )
    map_outputs = accums / totals[..., None]
    mixed_out = map_outputs[0] - lambdas[:, None, None] * map_outputs[1]
    scaled = (
        mixed_out
        * lax.rsqrt(jnp.mean(mixed_out * mixed_out, axis=-1, keepdims=True) + EPS_NORM)
        * head_gain
    )
    attended = scaled.astype(jnp.bfloat16)
    weight_piece = lax.all_gather(out_weight, "sp", axis=1, tiled=True)
    shaped = weight_piece.reshape(heads_here, V, weight_piece.shape[1])
    partial_terms = jnp.einsum("hqv,hvd->qd", attended, shaped, preferred_element_type=jnp.float32)
    summed = lax.psum_scatter(
        partial_terms.astype(jnp.bfloat16), "tp", scatter_dimension=0, tiled=True
    )
    return summed


def solution(mesh):
    in_specs = (
        P(("sp", "tp"), None),
        P("sp", "tp"),
        P("sp", "tp"),
        P("sp", "tp"),
        P("sp", "tp"),
        P("sp", "tp"),
        P("tp", "sp"),
        P("tp"),
        P(),
    )
    out_specs = P(("sp", "tp"), None)
    return jax.shard_map(
        on_device, mesh=mesh, in_specs=in_specs, out_specs=out_specs, check_vma=False
    )
```

profile of v0, /device:TPU:0, one launch (start us, length us, event | category | flops | bytes accessed | tf_op | source)
XLA Modules:
  0.0 554.6 jit_solution(14938328671323246360)
XLA Ops:
  6.5 0.7 all-gather.11.cloned.1.call-update
  7.3 0.7 all-gather.25.cloned.1.call-update
  8.1 0.7 all-gather.19.cloned.1.call-update
  8.8 0.5 all-gather.21.cloned.1.call-update
  9.4 0.5 all-gather.13.cloned.1.call-update
  10.5 23.7 %all-gather.11.cloned.1.call-done = bf16[256,4096]{1,0:T(8,128)(2,1)} async-done(((bf16[64,4096]{1,0:T(8,128)(2,1)}), bf16[256,4096]{1,0:T(8,128)(2,1)}) %all-gather.11.cloned.1.call-update) | async-done | bytes 2097168 | tf_op jit(solution)/shard_map/all_gather | solution.py:44
  34.2 74.9 %all-gather.25.cloned.1.call-done = bf16[4096,512]{1,0:T(8,128)(2,1)} async-done(((bf16[512,512]{1,0:T(8,128)(2,1)}), bf16[4096,512]{1,0:T(8,128)(2,1)}) %all-gather.25.cloned.1.call-update) | async-done | bytes 4194320 | tf_op jit(solution)/shard_map/all_gather | solution.py:52
  109.2 4.8 convolution_convert_fusion
  114.3 44.6 %all-gather.19.cloned.1.call-done = bf16[4096,256]{1,0:T(8,128)(2,1)} async-done(((bf16[512,256]{1,0:T(8,128)(2,1)}), bf16[4096,256]{1,0:T(8,128)(2,1)}) %all-gather.19.cloned.1.call-update) | async-done | bytes 2097168 | tf_op jit(solution)/shard_map/all_gather | solution.py:49
  159.0 2.5 fusion.74
  161.5 47.1 %all-gather.21.cloned.1.call-done = bf16[4096,256]{1,0:T(8,128)(2,1)} async-done(((bf16[512,256]{1,0:T(8,128)(2,1)}), bf16[4096,256]{1,0:T(8,128)(2,1)}) %all-gather.21.cloned.1.call-update) | async-done | bytes 2097168 | tf_op jit(solution)/shard_map/all_gather | solution.py:51
  208.6 2.5 fusion.75
  211.1 47.1 %all-gather.13.cloned.1.call-done = bf16[4096,256]{1,0:T(8,128)(2,1)} async-done(((bf16[512,256]{1,0:T(8,128)(2,1)}), bf16[4096,256]{1,0:T(8,128)(2,1)}) %all-gather.13.cloned.1.call-update) | async-done | bytes 2097168 | tf_op jit(solution)/shard_map/all_gather | solution.py:48
  258.2 2.5 fusion.72
  260.7 47.1 %all-gather.15.cloned.1.call-done = bf16[4096,256]{1,0:T(8,128)(2,1)} async-done(((bf16[512,256]{1,0:T(8,128)(2,1)}), bf16[4096,256]{1,0:T(8,128)(2,1)}) %all-gather.15.cloned.1.call-update) | async-done | bytes 2097168 | tf_op jit(solution)/shard_map/all_gather | solution.py:50
  307.8 2.5 fusion.73
  310.5 0.7 pad_maximum_fusion.7
  311.3 0.7 pad_maximum_fusion.5
  312.0 0.5 all-gather.29.cloned.1.call-update
  312.6 0.7 fusion.70
  313.3 1.2 slice_reduce_fusion.1
  316.8 40.8 %all-gather.27.cloned.1.call-done = bf16[2048,512]{1,0:T(8,128)(2,1)} async-done(((bf16[256,512]{1,0:T(8,128)(2,1)}), bf16[2048,512]{1,0:T(8,128)(2,1)}) %all-gather.27.cloned.1.call-update) | async-done | bytes 2097168 | tf_op jit(solution)/shard_map/all_gather | solution.py:73
  357.6 4.0 reshape.172
  361.6 36.0 %all-gather.23.cloned.1.call-done = bf16[2048,256]{0,1:T(8,128)(2,1)} async-done(((bf16[256,256]{0,1:T(8,128)(2,1)}), bf16[2048,256]{0,1:T(8,128)(2,1)}) %all-gather.23.cloned.1.call-update) | async-done | bytes 1048592 | tf_op jit(solution)/shard_map/all_gather | solution.py:72
  397.6 40.5 %all-gather.17.cloned.1.call-done = bf16[2048,256]{0,1:T(8,128)(2,1)} async-done(((bf16[256,256]{0,1:T(8,128)(2,1)}), bf16[2048,256]{0,1:T(8,128)(2,1)}) %all-gather.17.cloned.1.call-update) | async-done | bytes 1048592 | tf_op jit(solution)/shard_map/all_gather | solution.py:71
  438.1 8.6 %conditional.2 = (f32[2,2,128]{2,1,0:T(2,128)S(1)}, f32[2,2,128,256]{3,2,1,0:T(8,128)}) conditional(s32[]{:T(128)} %convert_element_type.52, () %tuple.21, (s32[2048]{0:T(1024)S(1)}, s32[128]{0:T(128)S(1)}, bf16[256,2,128]{0,2,1:T(8,128)(2,1)S(1)}, bf16[2048,2,128]{0,2,1:T(8,128)(2,1)}, bf16[256,2,128]{0,2,1:T(8,128)(2,1)S(1)}, ...), branch_computations={%region_2.3_spmd, %region_3.8_spmd} | conditional | flops 815136768 | bytes 35283528 | solution.py:129
  438.3 0.8 copy.20
  439.1 1.9 select_reduce_fusion.1
  441.0 0.8 copy.22
  441.8 2.1 fusion.5
  443.9 0.7 fusion.8
  444.6 0.7 fusion.11
  445.3 0.8 pad_maximum_fusion
  446.1 0.6 fusion.7
  446.7 10.4 %conditional.3 = (f32[2,2,128]{2,1,0:T(2,128)S(1)}, f32[2,2,128,256]{3,2,1,0:T(8,128)}) conditional(s32[]{:T(128)} %convert_element_type.57, () %tuple.23, (s32[2048]{0:T(1024)S(1)}, s32[128]{0:T(128)}, bf16[256,2,128]{0,2,1:T(8,128)(2,1)}, bf16[2048,2,128]{0,2,1:T(8,128)(2,1)}, bf16[256,2,128]{0,2,1:T(8,128)(2,1)S(1)}, ...), branch_computations={%region_9.10_spmd, %region_10.15_spmd} | conditional | flops 815136768 | bytes 35283528 | solution.py:129
  446.9 0.9 broadcast_compare_fusion.1
  447.8 1.7 copy.25
  449.5 1.9 select_reduce_fusion.3
  451.4 0.8 copy.27
  452.2 2.1 fusion.31
  454.3 0.7 fusion.34
  455.0 0.7 fusion.37
  455.7 0.8 pad_maximum_fusion.2
  456.5 0.6 fusion.33
  457.1 1.4 maximum_divide_fusion
  458.8 54.9 %all-gather.29.cloned.1.call-done = bf16[512,4096]{1,0:T(8,128)(2,1)} async-done(((bf16[512,512]{1,0:T(8,128)(2,1)}), bf16[512,4096]{1,0:T(8,128)(2,1)}) %all-gather.29.cloned.1.call-update) | async-done | bytes 4194320 | tf_op jit(solution)/shard_map/all_gather | solution.py:144
  513.7 4.8 fusion.52
  518.5 29.5 %reduce-scatter.2.cloned.1.call-done = bf16[64,4096]{1,0:T(8,128)(2,1)} async-done(((bf16[256,4096]{1,0:T(8,128)(2,1)}), bf16[64,4096]{1,0:T(8,128)(2,1)}) %reduce-scatter.2.cloned.1.call-update) | async-done | bytes 524304 | tf_op jit(solution)/shard_map/reduce_scatter | solution.py:147
  (49 shorter events, 2.0 us)
Async XLA Ops:
  6.5 27.7 %all-gather.11.cloned.1.call-start = ((), (), s32[]{:S(2)}) async-start(), calls=%async_computation.1 | async-start | bytes 2621440 | tf_op jit(solution)/shard_map/all_gather | solution.py:44
  7.3 101.9 %all-gather.25.cloned.1.call-start = ((), (), s32[]{:S(2)}) async-start(), calls=%async_computation.8 | async-start | bytes 4718592 | tf_op jit(solution)/shard_map/all_gather | solution.py:52
  8.0 150.9 %all-gather.19.cloned.1.call-start = ((), (), s32[]{:S(2)}) async-start(), calls=%async_computation.5 | async-start | bytes 2359296 | tf_op jit(solution)/shard_map/all_gather | solution.py:49
  8.7 199.9 %all-gather.21.cloned.1.call-start = ((), (), s32[]{:S(2)}) async-start(), calls=%async_computation.6 | async-start | bytes 2359296 | tf_op jit(solution)/shard_map/all_gather | solution.py:51
  9.3 248.9 %all-gather.13.cloned.1.call-start = ((), (), s32[]{:S(2)}) async-start(), calls=%async_computation.2 | async-start | bytes 2359296 | tf_op jit(solution)/shard_map/all_gather | solution.py:48
  9.9 297.9 %all-gather.15.cloned.1.call-start = ((), (), s32[]{:S(2)}) async-start(), calls=%async_computation.3 | async-start | bytes 2359296 | tf_op jit(solution)/shard_map/all_gather | solution.py:50
  10.5 347.1 %all-gather.27.cloned.1.call-start = ((), (), s32[]{:S(2)}) async-start(), calls=%async_computation.9 | async-start | bytes 2359296 | tf_op jit(solution)/shard_map/all_gather | solution.py:73
  34.2 124.7 %copy-start = (bf16[256,4096]{1,0:T(8,128)(2,1)S(1)}, bf16[256,4096]{1,0:T(8,128)(2,1)}, u32[]{:S(2)}) copy-start(bf16[256,4096]{1,0:T(8,128)(2,1)} %all-gather.11.cloned.1.call-done) | copy-start | bytes 6291460
  114.0 283.7 %all-gather.23.cloned.1.call-start = ((), (), s32[]{:S(2)}) async-start(), calls=%async_computation.7 | async-start | bytes 1179648 | tf_op jit(solution)/shard_map/all_gather | solution.py:72
  311.2 126.9 %all-gather.17.cloned.1.call-start = ((), (), s32[]{:S(2)}) async-start(), calls=%async_computation.4 | async-start | bytes 1179648 | tf_op jit(solution)/shard_map/all_gather | solution.py:71
  312.0 201.7 %all-gather.29.cloned.1.call-start = ((), (), s32[]{:S(2)}) async-start(), calls=%async_computation.10 | async-start | bytes 4718592 | tf_op jit(solution)/shard_map/all_gather | solution.py:144
  312.5 235.5 %reduce-scatter.2.cloned.1.call-start = ((), (), s32[]{:S(2)}) async-start(), calls=%async_computation.11 | async-start | bytes 2621440 | tf_op jit(solution)/shard_map/reduce_scatter | solution.py:147
  316.8 121.3 %copy-start.5 = (bf16[256,2,128]{0,2,1:T(8,128)(2,1)}, bf16[256,2,128]{0,2,1:T(8,128)(2,1)S(1)}, u32[]{:S(2)}) copy-start(bf16[256,2,128]{0,2,1:T(8,128)(2,1)S(1)} %pad_maximum_fusion.4) | copy-start | bytes 393220
  438.1 3.7 copy-start.1
  441.8 2.1 copy-start.3
  446.9 5.3 copy-start.2
  452.2 2.1 copy-start.4
  457.1 1.5 copy-start.6
  457.1 56.6 %copy-start.7 = (f32[256]{0:T(256)S(1)}, f32[256]{0:T(256)}, u32[]{:S(2)}) copy-start(f32[256]{0:T(256)} %param.21) | copy-start | bytes 3076
Sparse Core Ops, SparseCore 0:
  8.9 25.2 all-gather.10
  36.3 72.7 all-gather.24
  111.3 47.6 all-gather.18
  160.9 47.6 all-gather.20
  210.6 47.5 all-gather.12
  260.2 47.6 all-gather.14
  310.0 47.6 all-gather.26
  359.7 37.9 all-gather.22
  399.7 38.3 all-gather.16
  440.0 73.6 all-gather.28
  518.7 29.3 reduce-scatter.1
where the time goes:
time: 555 us
  waiting for transfers between devices  490 us (88%)
  matrix products  30.4 us (5%)
  between operations  15.7 us (3%)
  other arithmetic  9.28 us (2%)
  local copies, waits for them, and re-layouts  7.99 us (1%)
    all_gather x1, waiting for transfers between devices, on_device(): lax.all_gather(value_weight, 'sp', axis=0, tiled=True)  74.9 us
    all_gather x1, waiting for transfers between devices, on_device(): weight_piece = lax.all_gather(out_weight, 'sp', axis=1, tiled=True)  54.9 us
    all_gather x1, waiting for transfers between devices, on_device(): lax.all_gather(key_two, 'sp', axis=0, tiled=True)  47.1 us
    all_gather x1, waiting for transfers between devices, on_device(): lax.all_gather(key_one, 'sp', axis=0, tiled=True)  47.1 us
    all_gather x1, waiting for transfers between devices, on_device(): lax.all_gather(query_one, 'sp', axis=0, tiled=True)  47.1 us
    all_gather x1, waiting for transfers between devices, on_device(): lax.all_gather(query_two, 'sp', axis=0, tiled=True)  44.6 us
    all_gather x1, waiting for transfers between devices, on_device(): lax.all_gather(values, 'sp', axis=0, tiled=True)  40.8 us
    all_gather x1, waiting for transfers between devices, on_device(): lax.all_gather(k_one, 'sp', axis=0, tiled=True)  40.5 us
  transfers between devices with their start and end apart: 11, of which 11 were waited for; matrix products, arithmetic and copies ran while one was open for 8% of the time, Pallas kernels for 0%

commit v1 on v0

--- a/solution.py
+++ b/solution.py
@@ -7,6 +7,27 @@
 V = 256
 ROPE_BASE = 500000.0
 EPS_NORM = 0.02
+
+
+def gather_around(value, axis, dim):
+    size, index, width = (lax.axis_size(axis), lax.axis_index(axis), value.shape[dim])
+    right = [(i, (i + 1) % size) for i in range(size)]
+    left = [(i, (i - 1) % size) for i in range(size)]
+    out = jnp.zeros((*value.shape[:dim], size * width, *value.shape[dim + 1 :]), value.dtype)
+    out = lax.dynamic_update_slice_in_dim(out, value, index * width, axis=dim)
+    from_left = from_right = value
+    halfway = size // 2
+    for hop in range(1, halfway + 1):
+        from_left = lax.ppermute(from_left, axis, right)
+        out = lax.dynamic_update_slice_in_dim(
+            out, from_left, (index - hop) % size * width, axis=dim
+        )
+        if hop < size - halfway:
+            from_right = lax.ppermute(from_right, axis, left)
+            out = lax.dynamic_update_slice_in_dim(
+                out, from_right, (index + hop) % size * width, axis=dim
+            )
+    return out
 
 
 def rotate(values, positions):
@@ -48,7 +69,7 @@
         lax.all_gather(query_one, "sp", axis=0, tiled=True),
         lax.all_gather(query_two, "sp", axis=0, tiled=True),
         lax.all_gather(key_one, "sp", axis=0, tiled=True),
-        lax.all_gather(key_two, "sp", axis=0, tiled=True),
+        gather_around(key_two, "sp", 0),
         lax.all_gather(value_weight, "sp", axis=0, tiled=True),
     )
     projected = tuple(

time: 555 us -> 528 us (0.951)
  waiting for transfers between devices: 490 us -> 439 us
  starting transfers between devices: 0.39 us -> 16.8 us
  local copies, waits for them, and re-layouts: 7.99 us -> 15.2 us
    all_gather x1 -> x0, waiting for transfers between devices: 47.1 us -> none  [on_device(): lax.all_gather(key_two, 'sp', axis=0, tiled=True)]
    all_gather x1, waiting for transfers between devices: 44.6 us -> 6.41 us  [on_device(): lax.all_gather(query_two, 'sp', axis=0, tiled=True)]
    ppermute x0 -> x7, waiting for transfers between devices: none -> 32.8 us  [the longest x4 27.8 us: gather_around(): from_left = lax.ppermute(from_left, axis, right)]
    ppermute x0 -> x7, starting transfers between devices: none -> 16.4 us  [the longest x3 8.38 us: gather_around(): from_right = lax.ppermute(from_right, axis, left)]
    dynamic_update_slice x0 -> x8, local copies, waits for them, and re-layouts: none -> 5.76 us  [the longest x4 2.92 us: gather_around(): lax.dynamic_update_slice_in_dim(out, from_left, (index - hop) % size * wi...]
  transfers between devices with their start and end apart: 11 -> 17, of which waited for: 11 -> 17; matrix products, arithmetic and copies ran while one was open for 8% -> 9% of each run, Pallas kernels for 0% -> 0%
where the time goes in v1:
time: 528 us; the launch traced here: 527 us
  waiting for transfers between devices  439 us (83%)
  matrix products  30.3 us (6%)
  starting transfers between devices  16.8 us (3%)
  between operations  16.2 us (3%)
  local copies, waits for them, and re-layouts  15.2 us (3%)
  other arithmetic  9.2 us (2%)
    all_gather x1, waiting for transfers between devices, on_device(): lax.all_gather(value_weight, 'sp', axis=0, tiled=True)  75 us
    all_gather x1, waiting for transfers between devices, on_device(): weight_piece = lax.all_gather(out_weight, 'sp', axis=1, tiled=True)  55.8 us
    all_gather x1, waiting for transfers between devices, on_device(): lax.all_gather(query_one, 'sp', axis=0, tiled=True)  47.4 us
    all_gather x1, waiting for transfers between devices, on_device(): lax.all_gather(key_one, 'sp', axis=0, tiled=True)  47.1 us
    all_gather x1, waiting for transfers between devices, on_device(): lax.all_gather(k_one, 'sp', axis=0, tiled=True)  40.5 us
    all_gather x1, waiting for transfers between devices, on_device(): lax.all_gather(values, 'sp', axis=0, tiled=True)  40.4 us
    all_gather x1, waiting for transfers between devices, on_device(): lax.all_gather(k_two, 'sp', axis=0, tiled=True)  36 us
    reduce_scatter x1, waiting for transfers between devices, on_device(): lax.psum_scatter(partial_terms.astype(jnp.bfloat16), 'tp', scatter_dimens...  29.5 us
  transfers between devices with their start and end apart: 17, of which 17 were waited for; matrix products, arithmetic and copies ran while one was open for 9% of the time, Pallas kernels for 0%

profile of v1, /device:TPU:0, one launch (start us, length us, event | category | flops | bytes accessed | tf_op | source)
XLA Modules:
  0.0 527.0 jit_solution(6882979670573635744)
XLA Ops:
  10.0 24.2 %all-gather.10.cloned.1.call-done = bf16[256,4096]{1,0:T(8,128)(2,1)} async-done(((bf16[64,4096]{1,0:T(8,128)(2,1)}), bf16[256,4096]{1,0:T(8,128)(2,1)}) %all-gather.10.cloned.1.call-update) | async-done | bytes 2097168 | tf_op jit(solution)/shard_map/all_gather | solution.py:65
  34.2 75.0 %all-gather.22.cloned.1.call-done = bf16[4096,512]{1,0:T(8,128)(2,1)} async-done(((bf16[512,512]{1,0:T(8,128)(2,1)}), bf16[4096,512]{1,0:T(8,128)(2,1)}) %all-gather.22.cloned.1.call-update) | async-done | bytes 4194320 | tf_op jit(solution)/shard_map/all_gather | solution.py:73
  109.2 4.8 convolution_convert_fusion
  114.6 4.2 collective-permute-start.1
  118.8 10.4 %collective-permute-done = bf16[512,256]{1,0:T(8,128)(2,1)S(1)} collective-permute-done((bf16[512,256]{1,0:T(8,128)(2,1)S(1)}, bf16[512,256]{1,0:T(8,128)(2,1)S(1)}, u32[]{:S(2)}, u32[]{:S(2)}) %collective-permute-start) | collective-permute-done | bytes 262176 | tf_op jit(solution)/shard_map/ppermute | solution.py:21
  129.2 2.5 collective-permute-start.2
  132.0 2.2 collective-permute-done.1
  134.4 1.5 broadcast_in_dim.87
  136.6 5.3 %collective-permute-done.2 = bf16[512,256]{1,0:T(8,128)(2,1)S(1)} collective-permute-done((bf16[512,256]{1,0:T(8,128)(2,1)S(1)}, bf16[512,256]{1,0:T(8,128)(2,1)S(1)}, u32[]{:S(2)}, u32[]{:S(2)}) %collective-permute-start.2) | collective-permute-done | bytes 262176 | tf_op jit(solution)/shard_map/ppermute | solution.py:21
  141.9 2.5 collective-permute-start.4
  144.4 0.7 constant_dynamic-update-slice_fusion.6
  145.8 2.4 collective-permute-done.3
  148.2 3.9 collective-permute-start.5
  152.2 0.7 constant_dynamic-update-slice_fusion.4
  152.9 7.9 %collective-permute-done.4 = bf16[512,256]{1,0:T(8,128)(2,1)S(1)} collective-permute-done((bf16[512,256]{1,0:T(8,128)(2,1)S(1)}, bf16[512,256]{1,0:T(8,128)(2,1)S(1)}, u32[]{:S(2)}, u32[]{:S(2)}) %collective-permute-start.4) | collective-permute-done | bytes 262176 | tf_op jit(solution)/shard_map/ppermute | solution.py:21
  160.8 2.5 collective-permute-start.6
  164.0 0.7 constant_dynamic-update-slice_fusion.2
  165.9 4.2 collective-permute-done.6
  170.1 0.7 constant_dynamic-update-slice_fusion
  170.8 2.4 fusion.75
  173.2 6.4 %all-gather.18.cloned.1.call-done = bf16[4096,256]{1,0:T(8,128)(2,1)} async-done(((bf16[512,256]{1,0:T(8,128)(2,1)}), bf16[4096,256]{1,0:T(8,128)(2,1)}) %all-gather.18.cloned.1.call-update) | async-done | bytes 2097168 | tf_op jit(solution)/shard_map/all_gather | solution.py:70
  179.6 2.5 fusion.74
  182.2 47.4 %all-gather.12.cloned.1.call-done = bf16[4096,256]{1,0:T(8,128)(2,1)} async-done(((bf16[512,256]{1,0:T(8,128)(2,1)}), bf16[4096,256]{1,0:T(8,128)(2,1)}) %all-gather.12.cloned.1.call-update) | async-done | bytes 2097168 | tf_op jit(solution)/shard_map/all_gather | solution.py:69
  229.6 2.5 fusion.72
  232.1 47.1 %all-gather.14.cloned.1.call-done = bf16[4096,256]{1,0:T(8,128)(2,1)} async-done(((bf16[512,256]{1,0:T(8,128)(2,1)}), bf16[4096,256]{1,0:T(8,128)(2,1)}) %all-gather.14.cloned.1.call-update) | async-done | bytes 2097168 | tf_op jit(solution)/shard_map/all_gather | solution.py:71
  279.2 2.5 fusion.73
  284.8 1.2 slice_reduce_fusion.1
  288.5 40.4 %all-gather.24.cloned.1.call-done = bf16[2048,512]{1,0:T(8,128)(2,1)} async-done(((bf16[256,512]{1,0:T(8,128)(2,1)}), bf16[2048,512]{1,0:T(8,128)(2,1)}) %all-gather.24.cloned.1.call-update) | async-done | bytes 2097168 | tf_op jit(solution)/shard_map/all_gather | solution.py:94
  328.9 4.0 reshape.172
  332.9 36.0 %all-gather.20.cloned.1.call-done = bf16[2048,256]{0,1:T(8,128)(2,1)} async-done(((bf16[256,256]{0,1:T(8,128)(2,1)}), bf16[2048,256]{0,1:T(8,128)(2,1)}) %all-gather.20.cloned.1.call-update) | async-done | bytes 1048592 | tf_op jit(solution)/shard_map/all_gather | solution.py:93
  368.9 40.5 %all-gather.16.cloned.1.call-done = bf16[2048,256]{0,1:T(8,128)(2,1)} async-done(((bf16[256,256]{0,1:T(8,128)(2,1)}), bf16[2048,256]{0,1:T(8,128)(2,1)}) %all-gather.16.cloned.1.call-update) | async-done | bytes 1048592 | tf_op jit(solution)/shard_map/all_gather | solution.py:92
  409.4 8.6 %conditional.2 = (f32[2,2,128]{2,1,0:T(2,128)S(1)}, f32[2,2,128,256]{3,2,1,0:T(8,128)}) conditional(s32[]{:T(128)} %convert_element_type.52, () %tuple.21, (s32[2048]{0:T(1024)S(1)}, s32[128]{0:T(128)S(1)}, bf16[256,2,128]{0,2,1:T(8,128)(2,1)S(1)}, bf16[2048,2,128]{0,2,1:T(8,128)(2,1)}, bf16[256,2,128]{0,2,1:T(8,128)(2,1)S(1)}, ...), branch_computations={%region_2.3_spmd, %region_3.8_spmd} | conditional | flops 815136768 | bytes 35283528 | solution.py:150
  409.6 0.8 copy.20
  410.3 1.9 select_reduce_fusion.1
  412.3 0.8 copy.22
  413.0 2.1 fusion.5
  416.5 0.8 pad_maximum_fusion
  417.9 10.4 %conditional.3 = (f32[2,2,128]{2,1,0:T(2,128)S(1)}, f32[2,2,128,256]{3,2,1,0:T(8,128)}) conditional(s32[]{:T(128)} %convert_element_type.57, () %tuple.23, (s32[2048]{0:T(1024)S(1)}, s32[128]{0:T(128)}, bf16[256,2,128]{0,2,1:T(8,128)(2,1)}, bf16[2048,2,128]{0,2,1:T(8,128)(2,1)}, bf16[256,2,128]{0,2,1:T(8,128)(2,1)S(1)}, ...), branch_computations={%region_9.10_spmd, %region_10.15_spmd} | conditional | flops 815136768 | bytes 35283528 | solution.py:150
  418.1 0.9 broadcast_compare_fusion.1
  419.0 1.7 copy.25
  420.7 1.9 select_reduce_fusion.3
  422.6 0.8 copy.27
  423.4 2.1 fusion.31
  426.9 0.8 pad_maximum_fusion.2
  428.3 1.4 maximum_divide_fusion
  430.0 55.8 %all-gather.26.cloned.1.call-done = bf16[512,4096]{1,0:T(8,128)(2,1)} async-done(((bf16[512,512]{1,0:T(8,128)(2,1)}), bf16[512,4096]{1,0:T(8,128)(2,1)}) %all-gather.26.cloned.1.call-update) | async-done | bytes 4194320 | tf_op jit(solution)/shard_map/all_gather | solution.py:165
  485.8 4.8 fusion.52
  490.7 29.5 %reduce-scatter.2.cloned.1.call-done = bf16[64,4096]{1,0:T(8,128)(2,1)} async-done(((bf16[256,4096]{1,0:T(8,128)(2,1)}), bf16[64,4096]{1,0:T(8,128)(2,1)}) %reduce-scatter.2.cloned.1.call-update) | async-done | bytes 524304 | tf_op jit(solution)/shard_map/reduce_scatter | solution.py:168
  (71 shorter events, 15.3 us)
Async XLA Ops:
  6.5 27.7 %all-gather.10.cloned.1.call-start = ((), (), s32[]{:S(2)}) async-start(), calls=%async_computation.1 | async-start | bytes 2621440 | tf_op jit(solution)/shard_map/all_gather | solution.py:65
  7.3 101.9 %all-gather.22.cloned.1.call-start = ((), (), s32[]{:S(2)}) async-start(), calls=%async_computation.7 | async-start | bytes 4718592 | tf_op jit(solution)/shard_map/all_gather | solution.py:73
  8.0 171.6 %all-gather.18.cloned.1.call-start = ((), (), s32[]{:S(2)}) async-start(), calls=%async_computation.5 | async-start | bytes 2359296 | tf_op jit(solution)/shard_map/all_gather | solution.py:70
  8.7 220.9 %all-gather.12.cloned.1.call-start = ((), (), s32[]{:S(2)}) async-start(), calls=%async_computation.2 | async-start | bytes 2359296 | tf_op jit(solution)/shard_map/all_gather | solution.py:69
  9.3 269.9 %all-gather.14.cloned.1.call-start = ((), (), s32[]{:S(2)}) async-start(), calls=%async_computation.3 | async-start | bytes 2359296 | tf_op jit(solution)/shard_map/all_gather | solution.py:71
  9.9 104.1 %copy-start.6 = (bf16[512,256]{1,0:T(8,128)(2,1)S(1)}, bf16[512,256]{1,0:T(8,128)(2,1)}, u32[]{:S(2)}) copy-start(bf16[512,256]{1,0:T(8,128)(2,1)} %param.17) | copy-start | bytes 786436
  9.9 319.0 %all-gather.24.cloned.1.call-start = ((), (), s32[]{:S(2)}) async-start(), calls=%async_computation.8 | async-start | bytes 2359296 | tf_op jit(solution)/shard_map/all_gather | solution.py:94
  114.0 254.9 %all-gather.20.cloned.1.call-start = ((), (), s32[]{:S(2)}) async-start(), calls=%async_computation.6 | async-start | bytes 1179648 | tf_op jit(solution)/shard_map/all_gather | solution.py:93
  114.0 15.2 %collective-permute-start = (bf16[512,256]{1,0:T(8,128)(2,1)S(1)}, bf16[512,256]{1,0:T(8,128)(2,1)S(1)}, u32[]{:S(2)}, u32[]{:S(2)}) collective-permute-start(bf16[512,256]{1,0:T(8,128)(2,1)S(1)} %copy-done.6), channel_id=1, source_target_pairs={{0,4},{4,8},{8,12},{12,16},{16,20},{20,24},{24,28},{28,0},{1,5},{5... | collective-permute-start | bytes 786440 | tf_op jit(solution)/shard_map/ppermute | solution.py:21
  114.6 19.5 %collective-permute-start.1 = (bf16[512,256]{1,0:T(8,128)(2,1)S(1)}, bf16[512,256]{1,0:T(8,128)(2,1)S(1)}, u32[]{:S(2)}, u32[]{:S(2)}) collective-permute-start(bf16[512,256]{1,0:T(8,128)(2,1)S(1)} %copy-done.6), channel_id=1, source_target_pairs={{0,28},{4,0},{8,4},{12,8},{16,12},{20,16},{24,20},{28,24},{1,29},{... | collective-permute-start | bytes 786440 | tf_op jit(solution)/shard_map/ppermute | solution.py:26
  129.2 12.7 %collective-permute-start.2 = (bf16[512,256]{1,0:T(8,128)(2,1)S(1)}, bf16[512,256]{1,0:T(8,128)(2,1)S(1)}, u32[]{:S(2)}, u32[]{:S(2)}) collective-permute-start(bf16[512,256]{1,0:T(8,128)(2,1)S(1)} %collective-permute-done), channel_id=1, source_target_pairs={{0,4},{4,8},{8,12},{12,16},{16,20},{20,24},{24,28},{28,0},{1,5},{5... | collective-permute-start | bytes 786440 | tf_op jit(solution)/shard_map/ppermute | solution.py:21
  134.2 14.1 %collective-permute-start.3 = (bf16[512,256]{1,0:T(8,128)(2,1)S(1)}, bf16[512,256]{1,0:T(8,128)(2,1)S(1)}, u32[]{:S(2)}, u32[]{:S(2)}) collective-permute-start(bf16[512,256]{1,0:T(8,128)(2,1)S(1)} %collective-permute-done.1), channel_id=1, source_target_pairs={{0,28},{4,0},{8,4},{12,8},{16,12},{20,16},{24,20},{28,24},{1,29},{... | collective-permute-start | bytes 786440 | tf_op jit(solution)/shard_map/ppermute | solution.py:26
  135.9 34.9 %copy-start = (bf16[256,4096]{1,0:T(8,128)(2,1)S(1)}, bf16[256,4096]{1,0:T(8,128)(2,1)}, u32[]{:S(2)}) copy-start(bf16[256,4096]{1,0:T(8,128)(2,1)} %all-gather.10.cloned.1.call-done) | copy-start | bytes 6291460
  141.9 18.9 %collective-permute-start.4 = (bf16[512,256]{1,0:T(8,128)(2,1)S(1)}, bf16[512,256]{1,0:T(8,128)(2,1)S(1)}, u32[]{:S(2)}, u32[]{:S(2)}) collective-permute-start(bf16[512,256]{1,0:T(8,128)(2,1)S(1)} %collective-permute-done.2), channel_id=1, source_target_pairs={{0,4},{4,8},{8,12},{12,16},{16,20},{20,24},{24,28},{28,0},{1,5},{5... | collective-permute-start | bytes 786440 | tf_op jit(solution)/shard_map/ppermute | solution.py:21
  148.2 17.0 %collective-permute-start.5 = (bf16[512,256]{1,0:T(8,128)(2,1)S(1)}, bf16[512,256]{1,0:T(8,128)(2,1)S(1)}, u32[]{:S(2)}, u32[]{:S(2)}) collective-permute-start(bf16[512,256]{1,0:T(8,128)(2,1)S(1)} %collective-permute-done.3), channel_id=1, source_target_pairs={{0,28},{4,0},{8,4},{12,8},{16,12},{20,16},{24,20},{28,24},{1,29},{... | collective-permute-start | bytes 786440 | tf_op jit(solution)/shard_map/ppermute | solution.py:26
  160.8 9.3 %collective-permute-start.6 = (bf16[512,256]{1,0:T(8,128)(2,1)S(1)}, bf16[512,256]{1,0:T(8,128)(2,1)S(1)}, u32[]{:S(2)}, u32[]{:S(2)}) collective-permute-start(bf16[512,256]{1,0:T(8,128)(2,1)S(1)} %collective-permute-done.4), channel_id=1, source_target_pairs={{0,4},{4,8},{8,12},{12,16},{16,20},{20,24},{24,28},{28,0},{1,5},{5... | collective-permute-start | bytes 786440 | tf_op jit(solution)/shard_map/ppermute | solution.py:21
  282.6 126.8 %all-gather.16.cloned.1.call-start = ((), (), s32[]{:S(2)}) async-start(), calls=%async_computation.4 | async-start | bytes 1179648 | tf_op jit(solution)/shard_map/all_gather | solution.py:92
  283.3 202.5 %all-gather.26.cloned.1.call-start = ((), (), s32[]{:S(2)}) async-start(), calls=%async_computation.9 | async-start | bytes 4718592 | tf_op jit(solution)/shard_map/all_gather | solution.py:165
  284.1 236.1 %reduce-scatter.2.cloned.1.call-start = ((), (), s32[]{:S(2)}) async-start(), calls=%async_computation.10 | async-start | bytes 2621440 | tf_op jit(solution)/shard_map/reduce_scatter | solution.py:168
  288.5 120.9 %copy-start.5 = (bf16[256,2,128]{0,2,1:T(8,128)(2,1)}, bf16[256,2,128]{0,2,1:T(8,128)(2,1)S(1)}, u32[]{:S(2)}) copy-start(bf16[256,2,128]{0,2,1:T(8,128)(2,1)S(1)} %pad_maximum_fusion.4) | copy-start | bytes 393220
  409.4 3.7 copy-start.1
  413.0 2.1 copy-start.3
  418.1 5.3 %copy-start.2 = (bf16[2048,2,128]{0,2,1:T(8,128)(2,1)S(1)}, bf16[2048,2,128]{0,2,1:T(8,128)(2,1)}, u32[]{:S(2)}) copy-start(bf16[2048,2,128]{0,2,1:T(8,128)(2,1)} %get-tuple-element.85) | copy-start | bytes 3145732 | tf_op jit(solution)/shard_map/cond
  423.4 2.1 copy-start.4
  428.3 1.5 copy-start.7
  428.3 57.5 %copy-start.8 = (f32[256]{0:T(256)S(1)}, f32[256]{0:T(256)}, u32[]{:S(2)}) copy-start(f32[256]{0:T(256)} %param.21) | copy-start | bytes 3076
Sparse Core Ops, SparseCore 0:
  8.9 25.2 all-gather.9
  36.3 72.7 all-gather.21
  111.3 68.3 all-gather.17
  181.6 47.9 all-gather.11
  231.6 47.6 all-gather.13
  281.2 47.6 all-gather.23
  330.9 37.9 all-gather.19
  370.9 38.3 all-gather.15
  411.4 74.3 all-gather.25
  490.8 29.3 reduce-scatter.1
